TPU v7x, 32 devices: a whole 2x2x4 slice. The times are simulated.
32 devices in a mesh: ep: 8 (over z, x), tp: 4 (over y, core).
Axes of the slice: x: 2, y: 2, z: 4, core: 2. Of those that a mesh axis runs over, the one named last changes fastest.
Arguments:
- first_micro_values: bfloat16 [8192, 2048], P('ep', 'tp'), may hold values from -6 to 6
- group_state_maps: bfloat16 [2, 8192, 1024], P(None, 'ep', 'tp'), may hold values from -6 to 6
- gate_preactivation: bfloat16 [8192, 2048], P('ep', 'tp'), may hold values from -6 to 6
- step_preactivation: float32 [8192, 32], P('ep', 'tp'), may hold values from -5.7 to 5.7
- head_step_bias: float32 [32], P('tp'), may hold values from -12 to -3
- head_log_decay: float32 [32], P('tp'), may hold values from -12 to 1
- decay_increment: float32 [8192, 32], P('ep', 'tp'), may hold values from -1.4 to 0
- head_direct_gain: float32 [32], P('tp'), may hold values from 0.1 to 1.9
- convolution_value_taps: bfloat16 [4, 2048], P(None, 'tp'), may hold values from -3 to 3
- convolution_map_taps: bfloat16 [2, 4, 1024], P(None, None, 'tp'), may hold values from -3 to 3
- grouped_norm_gain: float32 [2048], P('tp'), may hold values from 0.1 to 1.9
- second_micro_tokens: bfloat16 [8192, 2048], P(('ep', 'tp')), may hold values from -6 to 6
- expert_norm_gain: float32 [2048], replicated, may hold values from 0.1 to 1.9
- routes: int32 [8192, 2], P(('ep', 'tp')), may hold values from 0 to 7, all different within a row; in each aligned block of 256 rows (0 to 255, 256 to 511, ...) at most 96 rows name the same one
- visit_weight: float32 [8192, 2], P(('ep', 'tp')), may hold values from 0.1 to 1
- gate_weight_table: bfloat16 [8, 2048, 1024], P('ep', None, 'tp'), may hold values from -0.125 to 0.125
- up_weight_table: bfloat16 [8, 2048, 1024], P('ep', None, 'tp'), may hold values from -0.125 to 0.125
- down_weight_table: bfloat16 [8, 2048, 1024], P('ep', None, 'tp'), may hold values from -0.1875 to 0.1875
Outputs:
- mixer_gated_output: bfloat16 [8192, 2048], P('ep', 'tp')
- routed_out: bfloat16 [8192, 2048], P(('ep', 'tp'))
Inputs may be any that keep to these rules, and one draw needn't show every extreme that they name: `routes`: A row names 2 different experts. In each aligned block of 256 rows (the rows of one device), no expert is named by more than 96 rows, a bound that some block reaches.
All inputs are finite; a program needn't handle non-finite values.
Results may differ from a plain program's by a relative error of at most 0.0071.
Values may be sent and summed in bfloat16 or wider, within the bound.
A program may use at most 128 MiB of HBM per device.

v0:
```python
import functools

import jax
import jax.numpy as jnp
from jax import lax
from jax.experimental import pallas as pl
from jax.experimental.pallas import tpu as pltpu
from jax.sharding import PartitionSpec as P


HEADDIM = 64
NSTATE = 128
BLOCK = 128
LANES = 128
HALO = 8
PHASES = 2
PAD_ROWS = 16

HIGHEST = lax.Precision.HIGHEST
EPSILON = 1e-05
F32 = jnp.float32
BF16 = jnp.bfloat16


def cost(flops, bytes_accessed):
    return pl.CostEstimate(flops=int(flops), bytes_accessed=int(bytes_accessed), transcendentals=0)


def params(*semantics):
    return pltpu.CompilerParams(dimension_semantics=semantics, vmem_limit_bytes=48 * 1024 * 1024)


def silu(x):
    return x / (1.0 + jnp.exp(-x))


def dot(a, b, dims=(((1,), (0,)), ((), ()))):
    return lax.dot_general(a, b, dims, preferred_element_type=F32)


def spread(columns, pair):
    rows = columns.shape[0]
    lane = lax.broadcasted_iota(jnp.int32, (rows, LANES), 1)
    first = jnp.broadcast_to(columns[:, 2 * pair : 2 * pair + 1], (rows, LANES))
    second = jnp.broadcast_to(columns[:, 2 * pair + 1 : 2 * pair + 2], (rows, LANES))
    return jnp.where(lane < HEADDIM, first, second)


def mixer_local_kernel(
    values_ref,
    maps_ref,
    before_ref,
    step_ref,
    increment_ref,
    bias_ref,
    rate_ref,
    direct_ref,
    value_taps_ref,
    map_taps_ref,
    y_ref,
    out_maps_ref,
    prefix_ref,
    end_ref,
    extended,
    state,
    total,
):
    block = pl.program_id(0)
    channels = values_ref.shape[1]
    width = maps_ref.shape[2]
    groups = width // NSTATE
    heads = step_ref.shape[1]
    per_group = heads // groups
    group_lanes = per_group * HEADDIM
    taps = value_taps_ref.shape[0]

    @pl.when(block == 0)
    def _():
        extended[0:HALO, :] = before_ref[...].astype(F32)
        state[...] = jnp.zeros_like(state)
        total[...] = jnp.zeros_like(total)

    extended[HALO:, 0:channels] = values_ref[...].astype(F32)
    extended[HALO:, channels : channels + width] = maps_ref[0].astype(F32)
    extended[HALO:, channels + width :] = maps_ref[1].astype(F32)

    def conv(start, stop, weights):
        summed = jnp.zeros((BLOCK, stop - start), F32)
        for j in range(taps):
            at = HALO - (taps - 1) + j
            summed = summed + weights[j : j + 1, :] * extended[at : at + BLOCK, start:stop]
        return silu(summed)

    step = jax.nn.softplus(step_ref[...] + bias_ref[...])
    log_decay = step * rate_ref[...] + increment_ref[...]
    row = lax.broadcasted_iota(jnp.int32, (BLOCK, BLOCK), 0)
    column = lax.broadcasted_iota(jnp.int32, (BLOCK, BLOCK), 1)
    causal = row >= column
    running = lax.dot_general(
        causal.astype(F32),
        log_decay,
        (((1,), (0,)), ((), ())),
        precision=HIGHEST,
        preferred_element_type=F32,
    )
    running_rows = jnp.transpose(running)
    block_total = running[BLOCK - 1 : BLOCK, :]
    decay_in = jnp.exp(running)
    to_end = jnp.exp(block_total - running)
    prefix_ref[...] = jnp.exp(running + total[...])
    total[...] = total[...] + block_total
    block_decay = jnp.exp(block_total)

    for g in range(groups):
        in_map = conv(
            channels + g * NSTATE, channels + (g + 1) * NSTATE, map_taps_ref[0, :, g * NSTATE : (g + 1) * NSTATE].astype(F32)
        ).astype(BF16)
        out_map = conv(
            channels + width + g * NSTATE,
            channels + width + (g + 1) * NSTATE,
            map_taps_ref[1, :, g * NSTATE : (g + 1) * NSTATE].astype(F32),
        ).astype(BF16)
        out_maps_ref[:, g * NSTATE : (g + 1) * NSTATE] = out_map
        scores = dot(out_map, in_map, (((1,), (1,)), ((), ())))
        scores = jnp.where(causal, scores, 0.0)
        for pair in range(per_group // 2):
            first = g * (per_group // 2) + pair
            lanes = slice(first * LANES, (first + 1) * LANES)
            inner = slice(pair * LANES, (pair + 1) * LANES)
            x = conv(lanes.start, lanes.stop, value_taps_ref[:, lanes].astype(F32))
            scaled = x * spread(step, first)
            scaled_low = scaled.astype(BF16)
            parts = []
            for h in (2 * first, 2 * first + 1):
                gap = running[:, h : h + 1] - running_rows[h : h + 1, :]
                weights = scores * jnp.exp(jnp.minimum(gap, 0.0))
                parts.append(dot(weights.astype(BF16), scaled_low))
            lane = lax.broadcasted_iota(jnp.int32, (BLOCK, LANES), 1)
            inside = jnp.where(lane < HEADDIM, parts[0], parts[1])
            entering = state[g, :, inner]
            carried = dot(out_map, entering.astype(BF16)) * spread(decay_in, first)
            y_ref[:, lanes] = inside + carried + x * spread(direct_ref[...], first)
            ending = (scaled * spread(to_end, first)).astype(BF16)
            added = dot(in_map, ending, (((0,), (0,)), ((), ())))
            state[g, :, inner] = entering * spread(block_decay, first) + added

    extended[0:HALO, :] = extended[BLOCK : BLOCK + HALO, :]

    @pl.when(block == pl.num_programs(0) - 1)
    def _():
        end_ref[0 : groups * NSTATE, :] = (
            state[...].reshape(groups * NSTATE, group_lanes).astype(BF16)
        )
        total_decay = jnp.exp(total[...])
        row_at = lax.broadcasted_iota(jnp.int32, (PAD_ROWS, LANES), 0)
        for pair in range(per_group // 2):
            decays = jnp.zeros((PAD_ROWS, LANES), F32)
            for g in range(groups):
                decay = spread(total_decay, g * (per_group // 2) + pair)
                decays = jnp.where(row_at == g, decay, decays)
            end_ref[groups * NSTATE :, pair * LANES : (pair + 1) * LANES] = decays.astype(BF16)


def merge_kernel(earlier_ref, later_ref, out_ref):
    split = later_ref.shape[0] - PAD_ROWS
    decays = later_ref[split:, :].astype(F32)
    for g in range(split // NSTATE):
        rows = slice(g * NSTATE, (g + 1) * NSTATE)
        merged = later_ref[rows, :].astype(F32) + decays[g : g + 1, :] * earlier_ref[
            rows, :
        ].astype(F32)
        out_ref[rows, :] = merged.astype(BF16)
    out_ref[split:, :] = (decays * earlier_ref[split:, :].astype(F32)).astype(BF16)


def mixer_finish_kernel(y_ref, out_maps_ref, prefix_ref, incoming_ref, gate_ref, gain_ref, out_ref):
    heads = prefix_ref.shape[1]
    groups = out_maps_ref.shape[1] // NSTATE
    per_group = heads // groups
    prefix = prefix_ref[...]
    for g in range(groups):
        out_map = out_maps_ref[:, g * NSTATE : (g + 1) * NSTATE]
        parts = []
        squares = 0.0
        for pair in range(per_group // 2):
            first = g * (per_group // 2) + pair
            lanes = slice(first * LANES, (first + 1) * LANES)
            incoming = incoming_ref[
                g * NSTATE : (g + 1) * NSTATE, pair * LANES : (pair + 1) * LANES
            ]
            y = y_ref[:, lanes] + dot(out_map, incoming) * spread(prefix, first)
            gated = y * silu(gate_ref[:, lanes].astype(F32))
            squares = squares + jnp.sum(gated * gated, axis=1, keepdims=True)
            parts.append((lanes, gated))
        scale = lax.rsqrt(squares / (per_group * HEADDIM) + EPSILON)
        for lanes, gated in parts:
            out_ref[:, lanes] = (gated * scale * gain_ref[:, lanes]).astype(BF16)


def dispatch_kernel(tokens_ref, gain_ref, routes_ref, *refs, capacity):
    target_ref = refs[-1]
    tokens = tokens_ref.shape[0]
    rows = refs[0].shape[0] * PHASES
    part = capacity // PHASES
    values = tokens_ref[...].astype(F32)
    centered = values - jnp.mean(values, axis=1, keepdims=True)
    variance = jnp.mean(centered * centered, axis=1, keepdims=True)
    normed = (centered * lax.rsqrt(variance + EPSILON) * gain_ref[...]).astype(BF16)
    routes = routes_ref[...]
    fanout = routes.shape[1]
    experts = lax.broadcasted_iota(jnp.int32, (tokens, LANES), 1)
    visits = jnp.zeros((tokens, LANES), F32)
    for k in range(fanout):
        visits = visits + (experts == routes[:, k : k + 1]).astype(F32)
    row = lax.broadcasted_iota(jnp.int32, (tokens, tokens), 0)
    column = lax.broadcasted_iota(jnp.int32, (tokens, tokens), 1)
    slots = dot((row > column).astype(F32).astype(BF16), visits.astype(BF16)).astype(jnp.int32)
    phase = jnp.zeros_like(slots)
    for late in range(1, PHASES):
        phase = phase + (slots >= late * part).astype(jnp.int32)
    slots = slots + phase * (rows // PHASES - part) + experts * part
    places = lax.broadcasted_iota(jnp.int32, (tokens, rows), 1)
    chosen = jnp.zeros((tokens, rows), F32)
    for k in range(fanout):
        target = jnp.sum(
            jnp.where(experts == routes[:, k : k + 1], slots.astype(F32), 0.0), axis=1, keepdims=True
        ).astype(jnp.int32)
        target_ref[:, k : k + 1] = target
        chosen = chosen + (places == target).astype(F32)
    chosen = chosen.astype(BF16)
    size = rows // PHASES
    for at, rows_ref in enumerate(refs[:-1]):
        picked = chosen[:, at * size : (at + 1) * size]
        rows_ref[...] = dot(picked, normed, (((0,), (0,)), ((), ()))).astype(BF16)


def combine_kernel(*refs, offset):
    returned_ref, target_ref, weight_ref = refs[:3]
    out_ref = refs[-1]
    tokens = target_ref.shape[0]
    rows = returned_ref.shape[0]
    places = lax.broadcasted_iota(jnp.int32, (tokens, rows), 1) + offset
    table = jnp.zeros((tokens, rows), F32)
    for k in range(target_ref.shape[1]):
        table = table + jnp.where(places == target_ref[:, k : k + 1], weight_ref[:, k : k + 1], 0.0)
    high = table.astype(BF16)
    low = (table - high.astype(F32)).astype(BF16)
    returned = returned_ref[...]
    summed = dot(high, returned) + dot(low, returned)
    if len(refs) > 4:
        summed = summed + refs[3][...]
    out_ref[...] = summed.astype(out_ref.dtype)


def hidden_kernel(*refs):
    rows_ref, hidden_ref = refs[0], refs[-1]
    count = (len(refs) - 2) // 2
    units = refs[1].shape[2]
    for at in range(count):
        rows = rows_ref[...]
        activated = silu(dot(rows, refs[1 + at][0]))
        hidden_ref[:, at * units : (at + 1) * units] = (
            activated * dot(rows, refs[1 + count + at][0])
        ).astype(BF16)


def down_kernel(*refs):
    hidden_ref, out_ref = refs[0], refs[-1]
    units = refs[1].shape[2]
    total = 0.0
    for at, down_ref in enumerate(refs[1:-1]):
        hidden = hidden_ref[:, at * units : (at + 1) * units]
        total = total + dot(hidden, down_ref[0], (((1,), (1,)), ((), ())))
    out_ref[...] = total.astype(BF16)


def whole(shape):
    return pl.BlockSpec(shape, lambda *_: (0,) * len(shape))


def shifted(block, axis, distance):
    devices = range(lax.axis_size(axis))
    route = [(i - distance, i) for i in devices if i - distance in devices]
    return lax.ppermute(block, axis, route)


def flipped(block, axis, bit):
    return lax.ppermute(block, axis, [(i, i ^ bit) for i in range(lax.axis_size(axis))])


def all_shards(block, axis):
    pieces = [block]
    bit = lax.axis_size(axis) // 2
    while bit:
        moved = []
        for piece in pieces:
            moved.append(flipped(piece, axis, bit))
        pieces = pieces + moved
        bit //= 2
    return pieces


def mixer_local(
    values,
    maps,
    before,
    step_preactivation,
    step_bias,
    log_rate,
    increment,
    direct,
    value_taps,
    map_taps,
):
    length, channels = values.shape
    heads = step_preactivation.shape[1]
    width = maps.shape[2]
    groups = width // NSTATE
    group_lanes = channels // groups
    taps = value_taps.shape[0]
    return pl.pallas_call(
        mixer_local_kernel,
        grid=(length // BLOCK,),
        in_specs=[
            pl.BlockSpec((BLOCK, channels), lambda i: (i, 0)),
            pl.BlockSpec((2, BLOCK, width), lambda i: (0, i, 0)),
            whole((HALO, channels + 2 * width)),
            pl.BlockSpec((BLOCK, heads), lambda i: (i, 0)),
            pl.BlockSpec((BLOCK, heads), lambda i: (i, 0)),
            whole((1, heads)),
            whole((1, heads)),
            whole((1, heads)),
            whole((taps, channels)),
            whole((2, taps, width)),
        ],
        out_specs=[
            pl.BlockSpec((BLOCK, channels), lambda i: (i, 0)),
            pl.BlockSpec((BLOCK, width), lambda i: (i, 0)),
            pl.BlockSpec((BLOCK, heads), lambda i: (i, 0)),
            whole((groups * NSTATE + PAD_ROWS, group_lanes)),
        ],
        out_shape=[
            jax.ShapeDtypeStruct((length, channels), F32),
            jax.ShapeDtypeStruct((length, width), BF16),
            jax.ShapeDtypeStruct((length, heads), F32),
            jax.ShapeDtypeStruct((groups * NSTATE + PAD_ROWS, group_lanes), BF16),
        ],
        scratch_shapes=[
            pltpu.VMEM((BLOCK + HALO, channels + 2 * width), F32),
            pltpu.VMEM((groups, NSTATE, group_lanes), F32),
            pltpu.VMEM((1, heads), F32),
        ],
        compiler_params=params("arbitrary"),
        cost_estimate=cost(15e9, 8e6),
        name="mixer_local",
    )(
        values,
        maps,
        before,
        step_preactivation,
        increment,
        step_bias[None],
        -jnp.exp(log_rate)[None],
        direct[None],
        value_taps,
        map_taps,
    )


def merged_states(earlier, later):
    return pl.pallas_call(
        merge_kernel,
        out_shape=jax.ShapeDtypeStruct(later.shape, later.dtype),
        compiler_params=params(),
        cost_estimate=cost(1e6, 4e5),
        name="merge",
    )(earlier, later)


def incoming_state(end):
    carried = shifted(end, "ep", 1)
    distance = 1
    while distance < lax.axis_size("ep") - 1:
        earlier = shifted(carried, "ep", distance)
        carried = merged_states(earlier, carried)
        distance *= 2
    return carried


def mixer_finish(y, out_maps, prefix, incoming, gate, gain):
    length, channels = y.shape
    tile = min(256, length)
    width = out_maps.shape[1]
    return pl.pallas_call(
        mixer_finish_kernel,
        grid=(length // tile,),
        in_specs=[
            pl.BlockSpec((tile, channels), lambda i: (i, 0)),
            pl.BlockSpec((tile, width), lambda i: (i, 0)),
            pl.BlockSpec((tile, prefix.shape[1]), lambda i: (i, 0)),
            whole(incoming.shape),
            pl.BlockSpec((tile, channels), lambda i: (i, 0)),
            whole((1, channels)),
        ],
        out_specs=pl.BlockSpec((tile, channels), lambda i: (i, 0)),
        out_shape=jax.ShapeDtypeStruct((length, channels), BF16),
        compiler_params=params("arbitrary"),
        cost_estimate=cost(4e9, 8e6),
        name="mixer_finish",
    )(y, out_maps, prefix, incoming, gate, gain[None])


def dispatched(tokens, gain, routes, rows, capacity):
    _, features = tokens.shape
    return pl.pallas_call(
        functools.partial(dispatch_kernel, capacity=capacity),
        out_shape=[
            *[jax.ShapeDtypeStruct((rows // PHASES, features), BF16)] * PHASES,
            jax.ShapeDtypeStruct(routes.shape, jnp.int32),
        ],
        compiler_params=params(),
        cost_estimate=cost(2e9, 5e6),
        name="dispatch",
    )(tokens, gain[None], routes)


def hidden_units(rows, gates, ups):
    count, features = rows.shape
    units = gates[0].shape[2] * len(gates)
    return pl.pallas_call(
        hidden_kernel,
        out_shape=jax.ShapeDtypeStruct((count, units), BF16),
        compiler_params=params(),
        cost_estimate=cost(4 * count * features * units, 1e7),
        name="hidden",
    )(rows, *gates, *ups)


def projected(hidden, downs):
    count, units = hidden.shape
    features, piece = downs[0].shape[1:]
    tile = min(512, features)
    return pl.pallas_call(
        down_kernel,
        grid=(features // tile,),
        in_specs=[whole(hidden.shape)]
        + [pl.BlockSpec((1, tile, piece), lambda i: (0, i, 0)) for d in downs],
        out_specs=pl.BlockSpec((count, tile), lambda i: (0, i)),
        out_shape=jax.ShapeDtypeStruct((count, features), BF16),
        compiler_params=params("arbitrary"),
        cost_estimate=cost(2 * count * features * units, 5e6),
        name="down",
    )(hidden, *downs)


def combined_rows(returned, target, weight, offset, partial, dtype):
    rows, features = returned.shape
    tile = min(512, features)
    tiles = pl.BlockSpec((target.shape[0], tile), lambda i: (0, i))
    partial = [] if partial is None else [partial]
    return pl.pallas_call(
        functools.partial(combine_kernel, offset=offset),
        grid=(features // tile,),
        in_specs=[
            pl.BlockSpec((rows, tile), lambda i: (0, i)),
            whole(target.shape),
            whole(weight.shape),
        ]
        + [tiles] * len(partial),
        out_specs=tiles,
        out_shape=jax.ShapeDtypeStruct((target.shape[0], features), dtype),
        compiler_params=params("arbitrary"),
        cost_estimate=cost(2e9, 4e6),
        name="combine",
    )(returned, target, weight, *partial)


def exchanged(rows, experts):
    count, features = rows.shape
    swapped = lax.all_to_all(
        rows.reshape(experts, count // experts, features),
        "ep",
        split_axis=0,
        concat_axis=0,
        tiled=True,
    )
    return swapped.reshape(count, features)


def body(
    first_micro_values,
    group_state_maps,
    gate_preactivation,
    step_preactivation,
    head_step_bias,
    head_log_decay,
    decay_increment,
    head_direct_gain,
    convolution_value_taps,
    convolution_map_taps,
    grouped_norm_gain,
    second_micro_tokens,
    expert_norm_gain,
    routes,
    visit_weight,
    gate_weight_table,
    up_weight_table,
    down_weight_table,
):
    tokens, _ = second_micro_tokens.shape
    length = first_micro_values.shape[0]
    experts = lax.axis_size("ep")
    capacity = max(2, 3 * tokens * routes.shape[1] // (2 * experts))
    size = experts * capacity // PHASES
    tail_rows = jnp.concatenate(
        [
            first_micro_values[length - HALO :],
            group_state_maps[0, length - HALO :],
            group_state_maps[1, length - HALO :],
        ],
        axis=1,
    )
    gates = all_shards(gate_weight_table, "tp")
    ups = all_shards(up_weight_table, "tp")
    downs = all_shards(down_weight_table, "tp")
    before = shifted(tail_rows, "ep", 1)
    *outgoing, target = dispatched(
        second_micro_tokens, expert_norm_gain, routes, experts * capacity, capacity
    )
    arrived = []
    for rows in outgoing:
        arrived.append(exchanged(rows, experts))
    y, out_maps, prefix, end = mixer_local(
        first_micro_values,
        group_state_maps,
        before,
        step_preactivation,
        head_step_bias,
        head_log_decay,
        decay_increment,
        head_direct_gain,
        convolution_value_taps,
        convolution_map_taps,
    )
    incoming = incoming_state(end)
    total = None
    for at, rows in enumerate(arrived):
        hidden = hidden_units(rows, gates, ups)
        results = projected(hidden, downs)
        returned = exchanged(results, experts)
        dtype = BF16 if at + 1 == PHASES else F32
        total = combined_rows(returned, target, visit_weight, at * size, total, dtype)
    mixer_out = mixer_finish(
        y, out_maps, prefix, incoming, gate_preactivation, grouped_norm_gain
    )
    return (mixer_out, total)


def solution(mesh):
    placed = (
        P("ep", "tp"),
        P(None, "ep", "tp"),
        P("ep", "tp"),
        P("ep", "tp"),
        P("tp"),
        P("tp"),
        P("ep", "tp"),
        P("tp"),
        P(None, "tp"),
        P(None, None, "tp"),
        P("tp"),
        P(("ep", "tp"), None),
        P(),
        P(("ep", "tp"), None),
        P(("ep", "tp"), None),
        P("ep", None, "tp"),
        P("ep", None, "tp"),
        P("ep", None, "tp"),
    )
    return jax.shard_map(
        body,
        mesh=mesh,
        in_specs=placed,
        out_specs=(P("ep", "tp"), P(("ep", "tp"), None)),
        check_vma=False,
    )
```

profile of v0, /device:TPU:0, one launch (start us, length us, event | category | flops | bytes accessed | tf_op | source)
XLA Modules:
  0.0 283.9 jit_solution(1872267622035381010)
XLA Ops:
  3.4 3.0 %dispatch.1 = (bf16[384,2048]{1,0:T(8,128)(2,1)S(1)}, bf16[384,2048]{1,0:T(8,128)(2,1)}, s32[256,2]{1,0:T(8,128)S(1)}) custom-call(bf16[256,2048]{1,0:T(8,128)(2,1)S(1)} %copy-done.5, f32[1,2048]{1,0:T(1,128)S(1)} %bitcast.20, s32[256,2]{1,0:T(8,128)S(1)} %copy.22.routes_ref), custom_call_target="tpu_custom_call" | custom-call | flops 2000000000 | bytes 5000000 | tf_op jit(solution)/shard_map/dispatch/pallas_call | solution.py:415
  6.3 44.2 %all_to_all.20 = bf16[8,48,2048]{2,1,0:T(8,128)(2,1)} all-to-all(bf16[8,48,2048]{2,1,0:T(8,128)(2,1)S(1)} %bitcast.19), channel_id=1, replica_groups=mesh['ep'=8,'tp'=4] {'ep'}, dimensions={0} | all-to-all | bytes 3145728 | tf_op jit(solution)/shard_map/all_to_all | solution.py:480
  50.5 4.4 %all-to-all-start = ((bf16[8,48,2048]{2,1,0:T(8,128)(2,1)}), bf16[8,48,2048]{2,1,0:T(8,128)(2,1)}, u32[]{:S(2)}, u32[]{:S(2)}) async-start(bf16[8,48,2048]{2,1,0:T(8,128)(2,1)} %bitcast.7), calls=%async_computation | async-start | bytes 3145728 | tf_op jit(solution)/shard_map/all_to_all | solution.py:480
  58.8 22.3 %collective-permute-done.5.refs_2_ = bf16[1,2048,256]{2,1,0:T(8,128)(2,1)S(1)} collective-permute-done((bf16[1,2048,256]{2,1,0:T(8,128)(2,1)S(1)}, bf16[1,2048,256]{2,1,0:T(8,128)(2,1)S(1)}, u32[]{:S(2)}, u32[]{:S(2)}) %collective-permute-start.5) | collective-permute-done | bytes 1048608 | tf_op jit(solution)/shard_map/ppermute | solution.py:288
  81.0 22.5 %collective-permute-done.8.refs_6_ = bf16[1,2048,256]{2,1,0:T(8,128)(2,1)S(1)} collective-permute-done((bf16[1,2048,256]{2,1,0:T(8,128)(2,1)}, bf16[1,2048,256]{2,1,0:T(8,128)(2,1)S(1)}, u32[]{:S(2)}, u32[]{:S(2)}) %collective-permute-start.8) | collective-permute-done | bytes 1048608 | tf_op jit(solution)/shard_map/ppermute | solution.py:288
  104.0 19.6 %collective-permute-done.11.refs_2_ = bf16[1,2048,256]{2,1,0:T(8,128)(2,1)S(1)} collective-permute-done((bf16[1,2048,256]{2,1,0:T(8,128)(2,1)S(1)}, bf16[1,2048,256]{2,1,0:T(8,128)(2,1)S(1)}, u32[]{:S(2)}, u32[]{:S(2)}) %collective-permute-start.11) | collective-permute-done | bytes 1048608 | tf_op jit(solution)/shard_map/ppermute | solution.py:288
  126.3 6.1 %hidden.3.refs_0_ = bf16[384,1024]{1,0:T(8,128)(2,1)S(1)} custom-call(bf16[384,2048]{1,0:T(8,128)(2,1)} %bitcast.26, bf16[1,2048,256]{2,1,0:T(8,128)(2,1)S(1)} %copy-done.7, bf16[1,2048,256]{2,1,0:T(8,128)(2,1)S(1)} %collective-permute-done.5.refs_2_, bf16[1,2048,256]{2,1,0:T(8,128)(2,1)S(1)} %collective-permute-done.6.refs_3_, ...), custom_call_target="tpu_custom_call" | custom-call | flops 3221225472 | bytes 10000000 | tf_op jit(solution)/shard_map/hidden/pallas_call | solution.py:430
  132.4 3.4 %down.3 = bf16[384,2048]{1,0:T(8,128)(2,1)} custom-call(bf16[384,1024]{1,0:T(8,128)(2,1)S(1)} %hidden.3.refs_0_, bf16[1,2048,256]{2,1,0:T(8,128)(2,1)S(1)} %copy-done, bf16[1,2048,256]{2,1,0:T(8,128)(2,1)S(1)} %collective-permute-done.11.refs_2_, bf16[1,2048,256]{2,1,0:T(8,128)(2,1)S(1)} %collective-permute-done.12.refs_3_, ...), custom_call_target="tpu_custom_call" | custom-call | flops 1610612736 | bytes 5000000 | tf_op jit(solution)/shard_map/down/pallas_call | solution.py:443
  137.0 5.6 %all-to-all-start.3 = ((bf16[8,48,2048]{2,1,0:T(8,128)(2,1)}), bf16[8,48,2048]{2,1,0:T(8,128)(2,1)}, u32[]{:S(2)}, u32[]{:S(2)}) async-start(bf16[8,48,2048]{2,1,0:T(8,128)(2,1)} %bitcast.25), calls=%async_computation.3 | async-start | bytes 3145728 | tf_op jit(solution)/shard_map/all_to_all | solution.py:480
  148.1 6.2 %hidden.2.refs_0_ = bf16[384,1024]{1,0:T(8,128)(2,1)S(1)} custom-call(bf16[384,2048]{1,0:T(8,128)(2,1)} %bitcast.8.refs_0_, bf16[1,2048,256]{2,1,0:T(8,128)(2,1)S(1)} %copy-done.8, bf16[1,2048,256]{2,1,0:T(8,128)(2,1)S(1)} %copy-done.11, bf16[1,2048,256]{2,1,0:T(8,128)(2,1)S(1)} %copy-done.13, bf16[1,2048,256]{2,1,0:T(8,128)(2,1)S(1)} %copy-done.15, ...), custom_call_target="tpu_custom_call" | custom-call | flops 3221225472 | bytes 10000000 | tf_op jit(solution)/shard_map/hidden/pallas_call | solution.py:430
  154.3 3.4 %down.2 = bf16[384,2048]{1,0:T(8,128)(2,1)} custom-call(bf16[384,1024]{1,0:T(8,128)(2,1)S(1)} %hidden.2.refs_0_, bf16[1,2048,256]{2,1,0:T(8,128)(2,1)S(1)} %copy-done, bf16[1,2048,256]{2,1,0:T(8,128)(2,1)S(1)} %collective-permute-done.11.refs_2_, bf16[1,2048,256]{2,1,0:T(8,128)(2,1)S(1)} %collective-permute-done.12.refs_3_, bf16[1,2048,256]{2,1,0:T(8,128)(2,1)S(1)} %copy-done.2), custom_call_target="tpu_custom_call" | custom-call | flops 1610612736 | bytes 5000000 | tf_op jit(solution)/shard_map/down/pallas_call | solution.py:443
  157.7 22.6 %all-to-all-done.3 = bf16[8,48,2048]{2,1,0:T(8,128)(2,1)} async-done(((bf16[8,48,2048]{2,1,0:T(8,128)(2,1)}), bf16[8,48,2048]{2,1,0:T(8,128)(2,1)}, u32[]{:S(2)}, u32[]{:S(2)}) %all-to-all-start.3) | async-done | bytes 1572896 | tf_op jit(solution)/shard_map/all_to_all | solution.py:480
  180.4 3.8 %all-to-all-start.1 = ((bf16[8,48,2048]{2,1,0:T(8,128)(2,1)}), bf16[8,48,2048]{2,1,0:T(8,128)(2,1)S(1)}, u32[]{:S(2)}, u32[]{:S(2)}) async-start(bf16[8,48,2048]{2,1,0:T(8,128)(2,1)} %bitcast.24), calls=%async_computation.1 | async-start | bytes 3145728 | tf_op jit(solution)/shard_map/all_to_all | solution.py:480
  184.2 3.9 %collective-permute-start = (bf16[8,1024]{1,0:T(8,128)(2,1)S(1)}, bf16[8,1024]{1,0:T(8,128)(2,1)S(1)}, u32[]{:S(2)}, u32[]{:S(2)}) collective-permute-start(bf16[8,1024]{1,0:T(8,128)(2,1)S(1)} %pad_maximum_fusion), channel_id=1, source_target_pairs={{0,4},{4,8},{8,12},{12,16},{16,20},{20,24},{24,28},{1,5},{5,9},{9,... | collective-permute-start | bytes 49160 | tf_op jit(solution)/shard_map/ppermute | solution.py:284
  188.5 9.0 %collective-permute-done.before_ref = bf16[8,1024]{1,0:T(8,128)(2,1)S(1)} collective-permute-done((bf16[8,1024]{1,0:T(8,128)(2,1)S(1)}, bf16[8,1024]{1,0:T(8,128)(2,1)S(1)}, u32[]{:S(2)}, u32[]{:S(2)}) %collective-permute-start) | collective-permute-done | bytes 16416 | tf_op jit(solution)/shard_map/ppermute | solution.py:284
  200.0 10.8 %mixer_local.1 = (f32[1024,512]{1,0:T(8,128)}, bf16[1024,256]{1,0:T(8,128)(2,1)S(1)}, f32[1024,8]{1,0:T(8,128)S(1)}, bf16[272,256]{1,0:T(8,128)(2,1)S(1)}) custom-call(bf16[1024,512]{1,0:T(8,128)(2,1)S(1)} %copy-done.3, bf16[2,1024,256]{2,1,0:T(8,128)(2,1)S(1)} %copy-done.4, bf16[8,1024]{1,0:T(8,128)(2,1)S(1)} %collective-permute-done.before_ref, ...), custom_call_target="tpu_custom_call" | custom-call | flops 15000000512 | bytes 8000000 | tf_op jit(solution)/shard_map/mixer_local/pallas_call | solution.py:321
  211.6 16.5 %collective-permute-start.1 = (bf16[272,256]{1,0:T(8,128)(2,1)S(1)}, bf16[272,256]{1,0:T(8,128)(2,1)S(1)}, u32[]{:S(2)}, u32[]{:S(2)}) collective-permute-start(bf16[272,256]{1,0:T(8,128)(2,1)S(1)} %get-tuple-element.12), channel_id=1, source_target_pairs={{0,4},{4,8},{8,12},{12,16},{16,20},{20,24},{24,28},{1,5},{5,9},{9,... | collective-permute-start | bytes 417800 | tf_op jit(solution)/shard_map/ppermute | solution.py:284
  230.7 5.3 %collective-permute-start.2 = (bf16[272,256]{1,0:T(8,128)(2,1)S(1)}, bf16[272,256]{1,0:T(8,128)(2,1)S(1)}, u32[]{:S(2)}, u32[]{:S(2)}) collective-permute-start(bf16[272,256]{1,0:T(8,128)(2,1)S(1)} %collective-permute-done.1.later_ref), channel_id=1, source_target_pairs={{0,4},{4,8},{8,12},{12,16},{16,20},{20,24},{24,28},{1,5},{5,9},{9,... | collective-permute-start | bytes 417800 | tf_op jit(solution)/shard_map/ppermute | solution.py:284
  236.0 2.6 collective-permute-done.2.earlier_ref
  238.6 12.1 %collective-permute-start.3 = (bf16[272,256]{1,0:T(8,128)(2,1)S(1)}, bf16[272,256]{1,0:T(8,128)(2,1)S(1)}, u32[]{:S(2)}, u32[]{:S(2)}) collective-permute-start(bf16[272,256]{1,0:T(8,128)(2,1)S(1)} %merge.3.later_ref), channel_id=1, source_target_pairs={{0,8},{4,12},{8,16},{12,20},{16,24},{20,28},{1,9},{5,13},{9,17},{1... | collective-permute-start | bytes 417800 | tf_op jit(solution)/shard_map/ppermute | solution.py:284
  253.3 9.1 %collective-permute-start.4 = (bf16[272,256]{1,0:T(8,128)(2,1)S(1)}, bf16[272,256]{1,0:T(8,128)(2,1)S(1)}, u32[]{:S(2)}, u32[]{:S(2)}) collective-permute-start(bf16[272,256]{1,0:T(8,128)(2,1)S(1)} %merge.4.later_ref), channel_id=1, source_target_pairs={{0,16},{4,20},{8,24},{12,28},{1,17},{5,21},{9,25},{13,29},{2,18},{... | collective-permute-start | bytes 417800 | tf_op jit(solution)/shard_map/ppermute | solution.py:284
  269.9 3.6 %mixer_finish.1 = bf16[1024,512]{1,0:T(8,128)(2,1)} custom-call(f32[1024,512]{1,0:T(8,128)S(1)} %copy-done.24, bf16[1024,256]{1,0:T(8,128)(2,1)S(1)} %copy-done.26, f32[1024,8]{1,0:T(8,128)S(1)} %copy-done.28, bf16[272,256]{1,0:T(8,128)(2,1)S(1)} %merge.5.incoming_ref, bf16[1024,512]{1,0:T(8,128)(2,1)S(1)} %copy-done.9, f32[1,512]{1,0:T(1,128)S(1)} %bitcast.21), custom_call_target="tpu_custom_call" | custom-call | flops 4000000000 | bytes 8000000 | tf_op jit(solution)/shard_map/mixer_finish/pallas_call | solution.py:394
  273.5 4.0 %combine.2.refs_3_ = f32[256,2048]{1,0:T(8,128)S(1)} custom-call(bf16[384,2048]{1,0:T(8,128)(2,1)} %bitcast.14.refs_0_, s32[256,2]{1,0:T(8,128)S(1)} %get-tuple-element.14.refs_1_, f32[256,2]{1,0:T(8,128)S(1)} %copy.24.refs_2_), custom_call_target="tpu_custom_call" | custom-call | flops 2000000000 | bytes 4000000 | tf_op jit(solution)/shard_map/combine/pallas_call | solution.py:461
  280.4 3.5 %combine.3 = bf16[256,2048]{1,0:T(8,128)(2,1)} custom-call(bf16[384,2048]{1,0:T(8,128)(2,1)S(1)} %bitcast.18, s32[256,2]{1,0:T(8,128)S(1)} %get-tuple-element.14.refs_1_, f32[256,2]{1,0:T(8,128)S(1)} %copy.24.refs_2_, f32[256,2048]{1,0:T(8,128)S(1)} %copy-done.23), custom_call_target="tpu_custom_call" | custom-call | flops 2000000000 | bytes 4000000 | tf_op jit(solution)/shard_map/combine/pallas_call | solution.py:461
  (104 shorter events, 35.7 us)
Async XLA Ops:
  50.5 86.5 %all-to-all-start = ((bf16[8,48,2048]{2,1,0:T(8,128)(2,1)}), bf16[8,48,2048]{2,1,0:T(8,128)(2,1)}, u32[]{:S(2)}, u32[]{:S(2)}) async-start(bf16[8,48,2048]{2,1,0:T(8,128)(2,1)} %bitcast.7), calls=%async_computation | async-start | bytes 3145728 | tf_op jit(solution)/shard_map/all_to_all | solution.py:480
  54.9 26.1 %collective-permute-start.5 = (bf16[1,2048,256]{2,1,0:T(8,128)(2,1)S(1)}, bf16[1,2048,256]{2,1,0:T(8,128)(2,1)S(1)}, u32[]{:S(2)}, u32[]{:S(2)}) collective-permute-start(bf16[1,2048,256]{2,1,0:T(8,128)(2,1)S(1)} %copy-done.6), channel_id=1, source_target_pairs={{0,2},{1,3},{2,0},{3,1},{4,6},{5,7},{6,4},{7,5},{8,10},{9,11},{10,... | collective-permute-start | bytes 3145736 | tf_op jit(solution)/shard_map/ppermute | solution.py:288
  56.5 47.0 %collective-permute-start.8 = (bf16[1,2048,256]{2,1,0:T(8,128)(2,1)}, bf16[1,2048,256]{2,1,0:T(8,128)(2,1)S(1)}, u32[]{:S(2)}, u32[]{:S(2)}) collective-permute-start(bf16[1,2048,256]{2,1,0:T(8,128)(2,1)} %refs_5_.3), channel_id=1, source_target_pairs={{0,2},{1,3},{2,0},{3,1},{4,6},{5,7},{6,4},{7,5},{8,10},{9,11},{10,... | collective-permute-start | bytes 3145736 | tf_op jit(solution)/shard_map/ppermute | solution.py:288
  57.0 46.5 %collective-permute-start.6 = (bf16[1,2048,256]{2,1,0:T(8,128)(2,1)S(1)}, bf16[1,2048,256]{2,1,0:T(8,128)(2,1)S(1)}, u32[]{:S(2)}, u32[]{:S(2)}) collective-permute-start(bf16[1,2048,256]{2,1,0:T(8,128)(2,1)S(1)} %copy-done.6), channel_id=1, source_target_pairs={{0,1},{1,0},{2,3},{3,2},{4,5},{5,4},{6,7},{7,6},{8,9},{9,8},{10,11... | collective-permute-start | bytes 3145736 | tf_op jit(solution)/shard_map/ppermute | solution.py:288
  57.0 66.6 %collective-permute-start.11 = (bf16[1,2048,256]{2,1,0:T(8,128)(2,1)S(1)}, bf16[1,2048,256]{2,1,0:T(8,128)(2,1)S(1)}, u32[]{:S(2)}, u32[]{:S(2)}) collective-permute-start(bf16[1,2048,256]{2,1,0:T(8,128)(2,1)S(1)} %copy-done), channel_id=1, source_target_pairs={{0,2},{1,3},{2,0},{3,1},{4,6},{5,7},{6,4},{7,5},{8,10},{9,11},{10,... | collective-permute-start | bytes 3145736 | tf_op jit(solution)/shard_map/ppermute | solution.py:288
  58.6 65.1 %collective-permute-start.9 = (bf16[1,2048,256]{2,1,0:T(8,128)(2,1)}, bf16[1,2048,256]{2,1,0:T(8,128)(2,1)S(1)}, u32[]{:S(2)}, u32[]{:S(2)}) collective-permute-start(bf16[1,2048,256]{2,1,0:T(8,128)(2,1)} %refs_5_.3), channel_id=1, source_target_pairs={{0,1},{1,0},{2,3},{3,2},{4,5},{5,4},{6,7},{7,6},{8,9},{9,8},{10,11... | collective-permute-start | bytes 3145736 | tf_op jit(solution)/shard_map/ppermute | solution.py:288
  81.0 51.4 %copy-start.10 = (bf16[1,2048,256]{2,1,0:T(8,128)(2,1)}, bf16[1,2048,256]{2,1,0:T(8,128)(2,1)S(1)}, u32[]{:S(2)}) copy-start(bf16[1,2048,256]{2,1,0:T(8,128)(2,1)S(1)} %collective-permute-done.5.refs_2_) | copy-start | bytes 3145732
  81.0 42.6 %collective-permute-start.7 = (bf16[1,2048,256]{2,1,0:T(8,128)(2,1)S(1)}, bf16[1,2048,256]{2,1,0:T(8,128)(2,1)S(1)}, u32[]{:S(2)}, u32[]{:S(2)}) collective-permute-start(bf16[1,2048,256]{2,1,0:T(8,128)(2,1)S(1)} %collective-permute-done.5.refs_2_), channel_id=1, source_target_pairs={{0,1},{1,0},{2,3},{3,2},{4,5},{5,4},{6,7},{7,6},{8,9},{9,8},{10,11... | collective-permute-start | bytes 3145736 | tf_op jit(solution)/shard_map/ppermute | solution.py:288
  103.5 20.2 %copy-start.32 = (bf16[1,2048,256]{2,1,0:T(8,128)(2,1)}, bf16[1,2048,256]{2,1,0:T(8,128)(2,1)S(1)}, u32[]{:S(2)}) copy-start(bf16[1,2048,256]{2,1,0:T(8,128)(2,1)S(1)} %collective-permute-done.8.refs_6_) | copy-start | bytes 3145732
  103.5 20.2 %collective-permute-start.10 = (bf16[1,2048,256]{2,1,0:T(8,128)(2,1)S(1)}, bf16[1,2048,256]{2,1,0:T(8,128)(2,1)S(1)}, u32[]{:S(2)}, u32[]{:S(2)}) collective-permute-start(bf16[1,2048,256]{2,1,0:T(8,128)(2,1)S(1)} %collective-permute-done.8.refs_6_), channel_id=1, source_target_pairs={{0,1},{1,0},{2,3},{3,2},{4,5},{5,4},{6,7},{7,6},{8,9},{9,8},{10,11... | collective-permute-start | bytes 3145736 | tf_op jit(solution)/shard_map/ppermute | solution.py:288
  103.5 28.9 %copy-start.12 = (bf16[1,2048,256]{2,1,0:T(8,128)(2,1)}, bf16[1,2048,256]{2,1,0:T(8,128)(2,1)S(1)}, u32[]{:S(2)}) copy-start(bf16[1,2048,256]{2,1,0:T(8,128)(2,1)S(1)} %collective-permute-done.6.refs_3_) | copy-start | bytes 3145732
  103.5 28.9 %collective-permute-start.12 = (bf16[1,2048,256]{2,1,0:T(8,128)(2,1)S(1)}, bf16[1,2048,256]{2,1,0:T(8,128)(2,1)S(1)}, u32[]{:S(2)}, u32[]{:S(2)}) collective-permute-start(bf16[1,2048,256]{2,1,0:T(8,128)(2,1)S(1)} %copy-done), channel_id=1, source_target_pairs={{0,1},{1,0},{2,3},{3,2},{4,5},{5,4},{6,7},{7,6},{8,9},{9,8},{10,11... | collective-permute-start | bytes 3145736 | tf_op jit(solution)/shard_map/ppermute | solution.py:288
  123.7 8.8 %collective-permute-start.13 = (bf16[1,2048,256]{2,1,0:T(8,128)(2,1)S(1)}, bf16[1,2048,256]{2,1,0:T(8,128)(2,1)S(1)}, u32[]{:S(2)}, u32[]{:S(2)}) collective-permute-start(bf16[1,2048,256]{2,1,0:T(8,128)(2,1)S(1)} %collective-permute-done.11.refs_2_), channel_id=1, source_target_pairs={{0,1},{1,0},{2,3},{3,2},{4,5},{5,4},{6,7},{7,6},{8,9},{9,8},{10,11... | collective-permute-start | bytes 3145736 | tf_op jit(solution)/shard_map/ppermute | solution.py:288
  137.0 43.3 %all-to-all-start.3 = ((bf16[8,48,2048]{2,1,0:T(8,128)(2,1)}), bf16[8,48,2048]{2,1,0:T(8,128)(2,1)}, u32[]{:S(2)}, u32[]{:S(2)}) async-start(bf16[8,48,2048]{2,1,0:T(8,128)(2,1)} %bitcast.25), calls=%async_computation.3 | async-start | bytes 3145728 | tf_op jit(solution)/shard_map/all_to_all | solution.py:480
  180.3 17.2 %copy-start.17 = (bf16[4,512]{1,0:T(4,128)(2,1)S(1)}, bf16[4,512]{1,0:T(4,128)(2,1)}, u32[]{:S(2)}) copy-start(bf16[4,512]{1,0:T(4,128)(2,1)} %value_taps_ref.1) | copy-start | bytes 12292
  180.4 98.5 %all-to-all-start.1 = ((bf16[8,48,2048]{2,1,0:T(8,128)(2,1)}), bf16[8,48,2048]{2,1,0:T(8,128)(2,1)S(1)}, u32[]{:S(2)}, u32[]{:S(2)}) async-start(bf16[8,48,2048]{2,1,0:T(8,128)(2,1)} %bitcast.24), calls=%async_computation.1 | async-start | bytes 3145728 | tf_op jit(solution)/shard_map/all_to_all | solution.py:480
  184.2 13.4 %collective-permute-start = (bf16[8,1024]{1,0:T(8,128)(2,1)S(1)}, bf16[8,1024]{1,0:T(8,128)(2,1)S(1)}, u32[]{:S(2)}, u32[]{:S(2)}) collective-permute-start(bf16[8,1024]{1,0:T(8,128)(2,1)S(1)} %pad_maximum_fusion), channel_id=1, source_target_pairs={{0,4},{4,8},{8,12},{12,16},{16,20},{20,24},{24,28},{1,5},{5,9},{9,... | collective-permute-start | bytes 49160 | tf_op jit(solution)/shard_map/ppermute | solution.py:284
  200.0 62.4 %copy-start.31 = (f32[256,2]{0,1:T(2,128)S(1)}, f32[256,2]{0,1:T(2,128)}, u32[]{:S(2)}) copy-start(f32[256,2]{0,1:T(2,128)} %param.32) | copy-start | bytes 6148
  200.0 65.0 %copy-start.19 = (f32[512]{0:T(512)S(1)}, f32[512]{0:T(512)}, u32[]{:S(2)}) copy-start(f32[512]{0:T(512)} %param.28) | copy-start | bytes 6148
  211.6 41.7 %copy-start.25 = (bf16[1024,256]{1,0:T(8,128)(2,1)}, bf16[1024,256]{1,0:T(8,128)(2,1)S(1)}, u32[]{:S(2)}) copy-start(bf16[1024,256]{1,0:T(8,128)(2,1)S(1)} %get-tuple-element.10.out_maps_ref) | copy-start | bytes 1572868
  211.6 19.1 %collective-permute-start.1 = (bf16[272,256]{1,0:T(8,128)(2,1)S(1)}, bf16[272,256]{1,0:T(8,128)(2,1)S(1)}, u32[]{:S(2)}, u32[]{:S(2)}) collective-permute-start(bf16[272,256]{1,0:T(8,128)(2,1)S(1)} %get-tuple-element.12), channel_id=1, source_target_pairs={{0,4},{4,8},{8,12},{12,16},{16,20},{20,24},{24,28},{1,5},{5,9},{9,... | collective-permute-start | bytes 417800 | tf_op jit(solution)/shard_map/ppermute | solution.py:284
  230.7 7.9 %collective-permute-start.2 = (bf16[272,256]{1,0:T(8,128)(2,1)S(1)}, bf16[272,256]{1,0:T(8,128)(2,1)S(1)}, u32[]{:S(2)}, u32[]{:S(2)}) collective-permute-start(bf16[272,256]{1,0:T(8,128)(2,1)S(1)} %collective-permute-done.1.later_ref), channel_id=1, source_target_pairs={{0,4},{4,8},{8,12},{12,16},{16,20},{20,24},{24,28},{1,5},{5,9},{9,... | collective-permute-start | bytes 417800 | tf_op jit(solution)/shard_map/ppermute | solution.py:284
  238.6 14.7 %collective-permute-start.3 = (bf16[272,256]{1,0:T(8,128)(2,1)S(1)}, bf16[272,256]{1,0:T(8,128)(2,1)S(1)}, u32[]{:S(2)}, u32[]{:S(2)}) collective-permute-start(bf16[272,256]{1,0:T(8,128)(2,1)S(1)} %merge.3.later_ref), channel_id=1, source_target_pairs={{0,8},{4,12},{8,16},{12,20},{16,24},{20,28},{1,9},{5,13},{9,17},{1... | collective-permute-start | bytes 417800 | tf_op jit(solution)/shard_map/ppermute | solution.py:284
  253.3 11.7 %collective-permute-start.4 = (bf16[272,256]{1,0:T(8,128)(2,1)S(1)}, bf16[272,256]{1,0:T(8,128)(2,1)S(1)}, u32[]{:S(2)}, u32[]{:S(2)}) collective-permute-start(bf16[272,256]{1,0:T(8,128)(2,1)S(1)} %merge.4.later_ref), channel_id=1, source_target_pairs={{0,16},{4,20},{8,24},{12,28},{1,17},{5,21},{9,25},{13,29},{2,18},{... | collective-permute-start | bytes 417800 | tf_op jit(solution)/shard_map/ppermute | solution.py:284
  (30 other events, 127.4 us)
where the time goes:
time: 285 us; the launch traced here: 284 us
  waiting for transfers between devices  106 us (37%)
  starting transfers between devices  65 us (23%)
  blocking collectives  44.2 us (16%)
  Pallas kernels  44 us (15%)
  local copies, waits for them, and re-layouts  23.6 us (8%)
    ppermute x9, waiting for transfers between devices, flipped(): lax.ppermute(block, axis, [(i, i ^ bit) for i in range(lax.axis_size(axis...  64.4 us
    ppermute x5, starting transfers between devices, shifted(): return lax.ppermute(block, axis, route)  46.9 us
    all_to_all x1, blocking collectives, exchanged(): lax.all_to_all(rows.reshape(experts, count // experts, features), 'ep', s...  44.2 us
    unnamed x76, local copies, waits for them, and re-layouts  22.9 us
    all_to_all x3, waiting for transfers between devices, exchanged(): lax.all_to_all(rows.reshape(experts, count // experts, features), 'ep', s...  22.6 us
    ppermute x5, waiting for transfers between devices, shifted(): return lax.ppermute(block, axis, route)  19.1 us
    all_to_all x3, starting transfers between devices, exchanged(): lax.all_to_all(rows.reshape(experts, count // experts, features), 'ep', s...  13.8 us
    pallas_call x2, Pallas kernels, hidden_units(): pl.pallas_call(hidden_kernel, out_shape=jax.ShapeDtypeStruct((count, unit...  12.2 us
  transfers between devices with their start and end apart: 17, of which 9 were waited for; matrix products, arithmetic and copies ran while one was open for 0% of the time, Pallas kernels for 13%

commit v1 on v0

--- a/solution.py
+++ b/solution.py
@@ -27,7 +27,7 @@
 
 
 def params(*semantics):
-    return pltpu.CompilerParams(dimension_semantics=semantics, vmem_limit_bytes=48 * 1024 * 1024)
+    return pltpu.CompilerParams(dimension_semantics=semantics, vmem_limit_bytes=62 * 1024 * 1024)
 
 
 def silu(x):
@@ -378,11 +378,11 @@
 
 
 def incoming_state(end):
-    carried = shifted(end, "ep", 1)
-    distance = 1
+    nearest = shifted(end, "ep", 1)
+    carried = merged_states(shifted(end, "ep", 2), nearest)
+    distance = 2
     while distance < lax.axis_size("ep") - 1:
-        earlier = shifted(carried, "ep", distance)
-        carried = merged_states(earlier, carried)
+        carried = merged_states(shifted(carried, "ep", distance), carried)
         distance *= 2
     return carried
 

time: 285 us -> 286 us (level)
  the two profiles are of different devices: /device:TPU:0 before, /device:TPU:26 now
where the time goes in v1:
time: 286 us; the launch traced here: 285 us
  waiting for transfers between devices  137 us (48%)
  Pallas kernels  65 us (23%)
  blocking collectives  40.7 us (14%)
  starting transfers between devices  30.1 us (11%)
  local copies, waits for them, and re-layouts  11 us (4%)
    ppermute x9, waiting for transfers between devices, flipped(): lax.ppermute(block, axis, [(i, i ^ bit) for i in range(lax.axis_size(axis...  64.2 us
    ppermute x5, waiting for transfers between devices, shifted(): return lax.ppermute(block, axis, route)  51.3 us
    all_to_all x1, blocking collectives, exchanged(): lax.all_to_all(rows.reshape(experts, count // experts, features), 'ep', s...  40.7 us
    all_to_all x3, waiting for transfers between devices, exchanged(): lax.all_to_all(rows.reshape(experts, count // experts, features), 'ep', s...  21.4 us
    all_to_all x3, starting transfers between devices, exchanged(): lax.all_to_all(rows.reshape(experts, count // experts, features), 'ep', s...  19.4 us
    pallas_call x2, Pallas kernels, hidden_units(): pl.pallas_call(hidden_kernel, out_shape=jax.ShapeDtypeStruct((count, unit...  16.5 us
    pallas_call x1, Pallas kernels, mixer_local(): pl.pallas_call(mixer_local_kernel, grid=(length // BLOCK,), in_specs=[pl....  12 us
    pallas_call x2, Pallas kernels, projected(): pl.pallas_call(down_kernel, grid=(features // tile,), in_specs=[whole(hid...  11.4 us
  transfers between devices with their start and end apart: 17, of which 9 were waited for; matrix products, arithmetic and copies ran while one was open for 1% of the time, Pallas kernels for 19%

profile of v1, /device:TPU:26, one launch (start us, length us, event | category | flops | bytes accessed | tf_op | source)
XLA Modules:
  0.0 285.1 jit_solution(16224320446622209054)
XLA Ops:
  2.1 4.3 %dispatch.1 = (bf16[384,2048]{1,0:T(8,128)(2,1)}, bf16[384,2048]{1,0:T(8,128)(2,1)}, s32[256,2]{1,0:T(8,128)}) custom-call(bf16[256,2048]{1,0:T(8,128)(2,1)} %tokens_ref.1, f32[1,2048]{1,0:T(1,128)} %bitcast.24, s32[256,2]{1,0:T(8,128)} %copy.22.routes_ref), custom_call_target="tpu_custom_call" | custom-call | flops 2000000000 | bytes 5000000 | tf_op jit(solution)/shard_map/dispatch/pallas_call | solution.py:415
  6.5 40.7 %all_to_all.20 = bf16[8,48,2048]{2,1,0:T(8,128)(2,1)} all-to-all(bf16[8,48,2048]{2,1,0:T(8,128)(2,1)} %bitcast.23), channel_id=1, replica_groups=mesh['ep'=8,'tp'=4] {'ep'}, dimensions={0} | all-to-all | bytes 3145728 | tf_op jit(solution)/shard_map/all_to_all | solution.py:480
  47.2 6.8 %all-to-all-start = ((bf16[8,48,2048]{2,1,0:T(8,128)(2,1)}), bf16[8,48,2048]{2,1,0:T(8,128)(2,1)}, u32[]{:S(2)}, u32[]{:S(2)}) async-start(bf16[8,48,2048]{2,1,0:T(8,128)(2,1)} %bitcast.21), calls=%async_computation | async-start | bytes 3145728 | tf_op jit(solution)/shard_map/all_to_all | solution.py:480
  57.7 22.2 %collective-permute-done.5.refs_2_ = bf16[1,2048,256]{2,1,0:T(8,128)(2,1)S(1)} collective-permute-done((bf16[1,2048,256]{2,1,0:T(8,128)(2,1)S(1)}, bf16[1,2048,256]{2,1,0:T(8,128)(2,1)S(1)}, u32[]{:S(2)}, u32[]{:S(2)}) %collective-permute-start.5) | collective-permute-done | bytes 1048608 | tf_op jit(solution)/shard_map/ppermute | solution.py:288
  80.0 22.5 %collective-permute-done.8.refs_6_ = bf16[1,2048,256]{2,1,0:T(8,128)(2,1)S(1)} collective-permute-done((bf16[1,2048,256]{2,1,0:T(8,128)(2,1)}, bf16[1,2048,256]{2,1,0:T(8,128)(2,1)S(1)}, u32[]{:S(2)}, u32[]{:S(2)}) %collective-permute-start.8) | collective-permute-done | bytes 1048608 | tf_op jit(solution)/shard_map/ppermute | solution.py:288
  103.0 19.5 %collective-permute-done.11.refs_2_ = bf16[1,2048,256]{2,1,0:T(8,128)(2,1)} collective-permute-done((bf16[1,2048,256]{2,1,0:T(8,128)(2,1)S(1)}, bf16[1,2048,256]{2,1,0:T(8,128)(2,1)}, u32[]{:S(2)}, u32[]{:S(2)}) %collective-permute-start.11) | collective-permute-done | bytes 1048608 | tf_op jit(solution)/shard_map/ppermute | solution.py:288
  124.7 8.2 %hidden.3.refs_0_ = bf16[384,1024]{1,0:T(8,128)(2,1)} custom-call(bf16[384,2048]{1,0:T(8,128)(2,1)} %bitcast.22, bf16[1,2048,256]{2,1,0:T(8,128)(2,1)} %refs_1_.6, bf16[1,2048,256]{2,1,0:T(8,128)(2,1)} %copy-done.10, bf16[1,2048,256]{2,1,0:T(8,128)(2,1)} %copy-done.12, bf16[1,2048,256]{2,1,0:T(8,128)(2,1)} %copy-done.14, bf16[1,2048,256]{2,1,0:T(8,128)(2,1)} %refs_5_.3, ...), custom_call_target="tpu_custom_call" | custom-call | flops 3221225472 | bytes 10000000 | tf_op jit(solution)/shard_map/hidden/pallas_call | solution.py:430
  133.0 5.8 %down.3 = bf16[384,2048]{1,0:T(8,128)(2,1)} custom-call(bf16[384,1024]{1,0:T(8,128)(2,1)} %hidden.3.refs_0_, bf16[1,2048,256]{2,1,0:T(8,128)(2,1)} %refs_1_.7, bf16[1,2048,256]{2,1,0:T(8,128)(2,1)} %collective-permute-done.11.refs_2_, bf16[1,2048,256]{2,1,0:T(8,128)(2,1)} %collective-permute-done.12.refs_3_, ...), custom_call_target="tpu_custom_call" | custom-call | flops 1610612736 | bytes 5000000 | tf_op jit(solution)/shard_map/down/pallas_call | solution.py:443
  138.7 6.0 %all-to-all-start.3 = ((bf16[8,48,2048]{2,1,0:T(8,128)(2,1)}), bf16[8,48,2048]{2,1,0:T(8,128)(2,1)S(1)}, u32[]{:S(2)}, u32[]{:S(2)}) async-start(bf16[8,48,2048]{2,1,0:T(8,128)(2,1)} %bitcast.19), calls=%async_computation.3 | async-start | bytes 3145728 | tf_op jit(solution)/shard_map/all_to_all | solution.py:480
  144.7 8.2 %hidden.2.refs_0_ = bf16[384,1024]{1,0:T(8,128)(2,1)} custom-call(bf16[384,2048]{1,0:T(8,128)(2,1)} %bitcast.8.refs_0_, bf16[1,2048,256]{2,1,0:T(8,128)(2,1)} %refs_1_.6, bf16[1,2048,256]{2,1,0:T(8,128)(2,1)} %copy-done.10, bf16[1,2048,256]{2,1,0:T(8,128)(2,1)} %copy-done.12, bf16[1,2048,256]{2,1,0:T(8,128)(2,1)} %copy-done.14, ...), custom_call_target="tpu_custom_call" | custom-call | flops 3221225472 | bytes 10000000 | tf_op jit(solution)/shard_map/hidden/pallas_call | solution.py:430
  153.0 5.7 %down.2 = bf16[384,2048]{1,0:T(8,128)(2,1)} custom-call(bf16[384,1024]{1,0:T(8,128)(2,1)} %hidden.2.refs_0_, bf16[1,2048,256]{2,1,0:T(8,128)(2,1)} %refs_1_.7, bf16[1,2048,256]{2,1,0:T(8,128)(2,1)} %collective-permute-done.11.refs_2_, bf16[1,2048,256]{2,1,0:T(8,128)(2,1)} %collective-permute-done.12.refs_3_, ...), custom_call_target="tpu_custom_call" | custom-call | flops 1610612736 | bytes 5000000 | tf_op jit(solution)/shard_map/down/pallas_call | solution.py:443
  158.7 21.4 %all-to-all-done.3 = bf16[8,48,2048]{2,1,0:T(8,128)(2,1)S(1)} async-done(((bf16[8,48,2048]{2,1,0:T(8,128)(2,1)}), bf16[8,48,2048]{2,1,0:T(8,128)(2,1)S(1)}, u32[]{:S(2)}, u32[]{:S(2)}) %all-to-all-start.3) | async-done | bytes 1572896 | tf_op jit(solution)/shard_map/all_to_all | solution.py:480
  181.2 6.6 %all-to-all-start.1 = ((bf16[8,48,2048]{2,1,0:T(8,128)(2,1)}), bf16[8,48,2048]{2,1,0:T(8,128)(2,1)}, u32[]{:S(2)}, u32[]{:S(2)}) async-start(bf16[8,48,2048]{2,1,0:T(8,128)(2,1)} %bitcast.18), calls=%async_computation.1 | async-start | bytes 3145728 | tf_op jit(solution)/shard_map/all_to_all | solution.py:480
  192.4 8.8 %collective-permute-done.before_ref = bf16[8,1024]{1,0:T(8,128)(2,1)S(1)} collective-permute-done((bf16[8,1024]{1,0:T(8,128)(2,1)S(1)}, bf16[8,1024]{1,0:T(8,128)(2,1)S(1)}, u32[]{:S(2)}, u32[]{:S(2)}) %collective-permute-start) | collective-permute-done | bytes 16416 | tf_op jit(solution)/shard_map/ppermute | solution.py:284
  201.8 12.0 %mixer_local.1 = (f32[1024,512]{1,0:T(8,128)}, bf16[1024,256]{1,0:T(8,128)(2,1)}, f32[1024,8]{1,0:T(8,128)}, bf16[272,256]{1,0:T(8,128)(2,1)}) custom-call(bf16[1024,512]{1,0:T(8,128)(2,1)} %values_ref.1, bf16[2,1024,256]{2,1,0:T(8,128)(2,1)} %maps_ref.1, bf16[8,1024]{1,0:T(8,128)(2,1)} %copy-done.16, f32[1024,8]{1,0:T(8,128)} %copy.20.step_ref, ...), custom_call_target="tpu_custom_call" | custom-call | flops 15000000512 | bytes 8000000 | tf_op jit(solution)/shard_map/mixer_local/pallas_call | solution.py:321
  216.4 12.7 %collective-permute-done.2.later_ref = bf16[272,256]{1,0:T(8,128)(2,1)S(1)} collective-permute-done((bf16[272,256]{1,0:T(8,128)(2,1)}, bf16[272,256]{1,0:T(8,128)(2,1)S(1)}, u32[]{:S(2)}, u32[]{:S(2)}) %collective-permute-start.2) | collective-permute-done | bytes 139296 | tf_op jit(solution)/shard_map/ppermute | solution.py:284
  229.1 4.1 %collective-permute-done.1.earlier_ref = bf16[272,256]{1,0:T(8,128)(2,1)S(1)} collective-permute-done((bf16[272,256]{1,0:T(8,128)(2,1)}, bf16[272,256]{1,0:T(8,128)(2,1)S(1)}, u32[]{:S(2)}, u32[]{:S(2)}) %collective-permute-start.1) | collective-permute-done | bytes 139296 | tf_op jit(solution)/shard_map/ppermute | solution.py:284
  233.9 1.7 merge.3.later_ref
  236.9 17.9 %collective-permute-done.3.earlier_ref = bf16[272,256]{1,0:T(8,128)(2,1)S(1)} collective-permute-done((bf16[272,256]{1,0:T(8,128)(2,1)}, bf16[272,256]{1,0:T(8,128)(2,1)S(1)}, u32[]{:S(2)}, u32[]{:S(2)}) %collective-permute-start.3) | collective-permute-done | bytes 139296 | tf_op jit(solution)/shard_map/ppermute | solution.py:284
  255.5 1.7 merge.4.later_ref
  259.2 7.7 %collective-permute-done.4.earlier_ref = bf16[272,256]{1,0:T(8,128)(2,1)S(1)} collective-permute-done((bf16[272,256]{1,0:T(8,128)(2,1)}, bf16[272,256]{1,0:T(8,128)(2,1)S(1)}, u32[]{:S(2)}, u32[]{:S(2)}) %collective-permute-start.4) | collective-permute-done | bytes 139296 | tf_op jit(solution)/shard_map/ppermute | solution.py:284
  269.3 5.6 %mixer_finish.1 = bf16[1024,512]{1,0:T(8,128)(2,1)} custom-call(f32[1024,512]{1,0:T(8,128)} %get-tuple-element.9.y_ref, bf16[1024,256]{1,0:T(8,128)(2,1)} %get-tuple-element.10.out_maps_ref, f32[1024,8]{1,0:T(8,128)} %get-tuple-element.11.prefix_ref, bf16[272,256]{1,0:T(8,128)(2,1)} %merge.5.incoming_ref, bf16[1024,512]{1,0:T(8,128)(2,1)} %gate_ref.1, ...), custom_call_target="tpu_custom_call" | custom-call | flops 4000000000 | bytes 8000000 | tf_op jit(solution)/shard_map/mixer_finish/pallas_call | solution.py:394
  274.9 5.0 %combine.2.refs_3_ = f32[256,2048]{1,0:T(8,128)} custom-call(bf16[384,2048]{1,0:T(8,128)(2,1)} %bitcast.20, s32[256,2]{1,0:T(8,128)} %get-tuple-element.14.refs_1_, f32[256,2]{1,0:T(8,128)} %copy.24.refs_2_), custom_call_target="tpu_custom_call" | custom-call | flops 2000000000 | bytes 4000000 | tf_op jit(solution)/shard_map/combine/pallas_call | solution.py:461
  279.9 5.2 %combine.3 = bf16[256,2048]{1,0:T(8,128)(2,1)} custom-call(bf16[384,2048]{1,0:T(8,128)(2,1)} %bitcast.10.refs_0_, s32[256,2]{1,0:T(8,128)} %get-tuple-element.14.refs_1_, f32[256,2]{1,0:T(8,128)} %copy.24.refs_2_, f32[256,2048]{1,0:T(8,128)} %combine.2.refs_3_), custom_call_target="tpu_custom_call" | custom-call | flops 2000000000 | bytes 4000000 | tf_op jit(solution)/shard_map/combine/pallas_call | solution.py:461
  (68 shorter events, 24.0 us)
Async XLA Ops:
  47.2 91.6 %all-to-all-start = ((bf16[8,48,2048]{2,1,0:T(8,128)(2,1)}), bf16[8,48,2048]{2,1,0:T(8,128)(2,1)}, u32[]{:S(2)}, u32[]{:S(2)}) async-start(bf16[8,48,2048]{2,1,0:T(8,128)(2,1)} %bitcast.21), calls=%async_computation | async-start | bytes 3145728 | tf_op jit(solution)/shard_map/all_to_all | solution.py:480
  53.9 26.0 %collective-permute-start.5 = (bf16[1,2048,256]{2,1,0:T(8,128)(2,1)S(1)}, bf16[1,2048,256]{2,1,0:T(8,128)(2,1)S(1)}, u32[]{:S(2)}, u32[]{:S(2)}) collective-permute-start(bf16[1,2048,256]{2,1,0:T(8,128)(2,1)S(1)} %copy-done.9), channel_id=1, source_target_pairs={{0,2},{1,3},{2,0},{3,1},{4,6},{5,7},{6,4},{7,5},{8,10},{9,11},{10,... | collective-permute-start | bytes 3145736 | tf_op jit(solution)/shard_map/ppermute | solution.py:288
  55.5 47.0 %collective-permute-start.8 = (bf16[1,2048,256]{2,1,0:T(8,128)(2,1)}, bf16[1,2048,256]{2,1,0:T(8,128)(2,1)S(1)}, u32[]{:S(2)}, u32[]{:S(2)}) collective-permute-start(bf16[1,2048,256]{2,1,0:T(8,128)(2,1)} %refs_5_.3), channel_id=1, source_target_pairs={{0,2},{1,3},{2,0},{3,1},{4,6},{5,7},{6,4},{7,5},{8,10},{9,11},{10,... | collective-permute-start | bytes 3145736 | tf_op jit(solution)/shard_map/ppermute | solution.py:288
  56.0 46.5 %collective-permute-start.6 = (bf16[1,2048,256]{2,1,0:T(8,128)(2,1)S(1)}, bf16[1,2048,256]{2,1,0:T(8,128)(2,1)S(1)}, u32[]{:S(2)}, u32[]{:S(2)}) collective-permute-start(bf16[1,2048,256]{2,1,0:T(8,128)(2,1)S(1)} %copy-done.9), channel_id=1, source_target_pairs={{0,1},{1,0},{2,3},{3,2},{4,5},{5,4},{6,7},{7,6},{8,9},{9,8},{10,11... | collective-permute-start | bytes 3145736 | tf_op jit(solution)/shard_map/ppermute | solution.py:288
  56.0 66.5 %collective-permute-start.11 = (bf16[1,2048,256]{2,1,0:T(8,128)(2,1)S(1)}, bf16[1,2048,256]{2,1,0:T(8,128)(2,1)}, u32[]{:S(2)}, u32[]{:S(2)}) collective-permute-start(bf16[1,2048,256]{2,1,0:T(8,128)(2,1)S(1)} %copy-done), channel_id=1, source_target_pairs={{0,2},{1,3},{2,0},{3,1},{4,6},{5,7},{6,4},{7,5},{8,10},{9,11},{10,... | collective-permute-start | bytes 3145736 | tf_op jit(solution)/shard_map/ppermute | solution.py:288
  57.5 64.9 %collective-permute-start.9 = (bf16[1,2048,256]{2,1,0:T(8,128)(2,1)}, bf16[1,2048,256]{2,1,0:T(8,128)(2,1)S(1)}, u32[]{:S(2)}, u32[]{:S(2)}) collective-permute-start(bf16[1,2048,256]{2,1,0:T(8,128)(2,1)} %refs_5_.3), channel_id=1, source_target_pairs={{0,1},{1,0},{2,3},{3,2},{4,5},{5,4},{6,7},{7,6},{8,9},{9,8},{10,11... | collective-permute-start | bytes 3145736 | tf_op jit(solution)/shard_map/ppermute | solution.py:288
  80.0 42.5 %copy-start.10 = (bf16[1,2048,256]{2,1,0:T(8,128)(2,1)}, bf16[1,2048,256]{2,1,0:T(8,128)(2,1)S(1)}, u32[]{:S(2)}) copy-start(bf16[1,2048,256]{2,1,0:T(8,128)(2,1)S(1)} %collective-permute-done.5.refs_2_) | copy-start | bytes 3145732
  80.0 42.5 %collective-permute-start.7 = (bf16[1,2048,256]{2,1,0:T(8,128)(2,1)S(1)}, bf16[1,2048,256]{2,1,0:T(8,128)(2,1)S(1)}, u32[]{:S(2)}, u32[]{:S(2)}) collective-permute-start(bf16[1,2048,256]{2,1,0:T(8,128)(2,1)S(1)} %collective-permute-done.5.refs_2_), channel_id=1, source_target_pairs={{0,1},{1,0},{2,3},{3,2},{4,5},{5,4},{6,7},{7,6},{8,9},{9,8},{10,11... | collective-permute-start | bytes 3145736 | tf_op jit(solution)/shard_map/ppermute | solution.py:288
  102.4 20.0 %copy-start.11 = (bf16[1,2048,256]{2,1,0:T(8,128)(2,1)}, bf16[1,2048,256]{2,1,0:T(8,128)(2,1)S(1)}, u32[]{:S(2)}) copy-start(bf16[1,2048,256]{2,1,0:T(8,128)(2,1)S(1)} %collective-permute-done.8.refs_6_) | copy-start | bytes 3145732
  102.4 20.0 %collective-permute-start.10 = (bf16[1,2048,256]{2,1,0:T(8,128)(2,1)S(1)}, bf16[1,2048,256]{2,1,0:T(8,128)(2,1)S(1)}, u32[]{:S(2)}, u32[]{:S(2)}) collective-permute-start(bf16[1,2048,256]{2,1,0:T(8,128)(2,1)S(1)} %collective-permute-done.8.refs_6_), channel_id=1, source_target_pairs={{0,1},{1,0},{2,3},{3,2},{4,5},{5,4},{6,7},{7,6},{8,9},{9,8},{10,11... | collective-permute-start | bytes 3145736 | tf_op jit(solution)/shard_map/ppermute | solution.py:288
  102.4 20.0 %copy-start.12 = (bf16[1,2048,256]{2,1,0:T(8,128)(2,1)}, bf16[1,2048,256]{2,1,0:T(8,128)(2,1)S(1)}, u32[]{:S(2)}) copy-start(bf16[1,2048,256]{2,1,0:T(8,128)(2,1)S(1)} %collective-permute-done.6.refs_3_) | copy-start | bytes 3145732
  102.5 30.5 %collective-permute-start.12 = (bf16[1,2048,256]{2,1,0:T(8,128)(2,1)S(1)}, bf16[1,2048,256]{2,1,0:T(8,128)(2,1)}, u32[]{:S(2)}, u32[]{:S(2)}) collective-permute-start(bf16[1,2048,256]{2,1,0:T(8,128)(2,1)S(1)} %copy-done), channel_id=1, source_target_pairs={{0,1},{1,0},{2,3},{3,2},{4,5},{5,4},{6,7},{7,6},{8,9},{9,8},{10,11... | collective-permute-start | bytes 3145736 | tf_op jit(solution)/shard_map/ppermute | solution.py:288
  122.4 10.6 %collective-permute-start.13 = (bf16[1,2048,256]{2,1,0:T(8,128)(2,1)}, bf16[1,2048,256]{2,1,0:T(8,128)(2,1)}, u32[]{:S(2)}, u32[]{:S(2)}) collective-permute-start(bf16[1,2048,256]{2,1,0:T(8,128)(2,1)} %collective-permute-done.11.refs_2_), channel_id=1, source_target_pairs={{0,1},{1,0},{2,3},{3,2},{4,5},{5,4},{6,7},{7,6},{8,9},{9,8},{10,11... | collective-permute-start | bytes 3145736 | tf_op jit(solution)/shard_map/ppermute | solution.py:288
  138.7 41.3 %all-to-all-start.3 = ((bf16[8,48,2048]{2,1,0:T(8,128)(2,1)}), bf16[8,48,2048]{2,1,0:T(8,128)(2,1)S(1)}, u32[]{:S(2)}, u32[]{:S(2)}) async-start(bf16[8,48,2048]{2,1,0:T(8,128)(2,1)} %bitcast.19), calls=%async_computation.3 | async-start | bytes 3145728 | tf_op jit(solution)/shard_map/all_to_all | solution.py:480
  180.1 9.7 %copy-start.17 = (f32[8]{0:T(128)S(1)}, f32[8]{0:T(128)}, u32[]{:S(2)}) copy-start(f32[8]{0:T(128)} %param.23) | copy-start | bytes 100
  180.1 10.3 %copy-start.6 = (f32[1024,8]{0,1:T(8,128)S(1)}, f32[1024,8]{0,1:T(8,128)}, u32[]{:S(2)}) copy-start(f32[1024,8]{0,1:T(8,128)} %param.21) | copy-start | bytes 98308
  180.1 11.3 %copy-start.7 = (f32[1024,8]{0,1:T(8,128)S(1)}, f32[1024,8]{0,1:T(8,128)}, u32[]{:S(2)}) copy-start(f32[1024,8]{0,1:T(8,128)} %param.24) | copy-start | bytes 98308
  181.2 98.7 %all-to-all-start.1 = ((bf16[8,48,2048]{2,1,0:T(8,128)(2,1)}), bf16[8,48,2048]{2,1,0:T(8,128)(2,1)}, u32[]{:S(2)}, u32[]{:S(2)}) async-start(bf16[8,48,2048]{2,1,0:T(8,128)(2,1)} %bitcast.18), calls=%async_computation.1 | async-start | bytes 3145728 | tf_op jit(solution)/shard_map/all_to_all | solution.py:480
  188.5 12.7 %collective-permute-start = (bf16[8,1024]{1,0:T(8,128)(2,1)S(1)}, bf16[8,1024]{1,0:T(8,128)(2,1)S(1)}, u32[]{:S(2)}, u32[]{:S(2)}) collective-permute-start(bf16[8,1024]{1,0:T(8,128)(2,1)S(1)} %pad_maximum_fusion), channel_id=1, source_target_pairs={{0,4},{4,8},{8,12},{12,16},{16,20},{20,24},{24,28},{1,5},{5,9},{9,... | collective-permute-start | bytes 49160 | tf_op jit(solution)/shard_map/ppermute | solution.py:284
  201.8 56.6 %copy-start.8 = (f32[256,2]{0,1:T(2,128)S(1)}, f32[256,2]{0,1:T(2,128)}, u32[]{:S(2)}) copy-start(f32[256,2]{0,1:T(2,128)} %param.32) | copy-start | bytes 6148
  213.8 15.3 %collective-permute-start.2 = (bf16[272,256]{1,0:T(8,128)(2,1)}, bf16[272,256]{1,0:T(8,128)(2,1)S(1)}, u32[]{:S(2)}, u32[]{:S(2)}) collective-permute-start(bf16[272,256]{1,0:T(8,128)(2,1)} %get-tuple-element.12), channel_id=1, source_target_pairs={{0,4},{4,8},{8,12},{12,16},{16,20},{20,24},{24,28},{1,5},{5,9},{9,... | collective-permute-start | bytes 417800 | tf_op jit(solution)/shard_map/ppermute | solution.py:284
  215.1 18.1 %collective-permute-start.1 = (bf16[272,256]{1,0:T(8,128)(2,1)}, bf16[272,256]{1,0:T(8,128)(2,1)S(1)}, u32[]{:S(2)}, u32[]{:S(2)}) collective-permute-start(bf16[272,256]{1,0:T(8,128)(2,1)} %get-tuple-element.12), channel_id=1, source_target_pairs={{0,8},{4,12},{8,16},{12,20},{16,24},{20,28},{1,9},{5,13},{9,17},{1... | collective-permute-start | bytes 417800 | tf_op jit(solution)/shard_map/ppermute | solution.py:284
  235.6 19.2 %collective-permute-start.3 = (bf16[272,256]{1,0:T(8,128)(2,1)}, bf16[272,256]{1,0:T(8,128)(2,1)S(1)}, u32[]{:S(2)}, u32[]{:S(2)}) collective-permute-start(bf16[272,256]{1,0:T(8,128)(2,1)} %merge.3.later_ref), channel_id=1, source_target_pairs={{0,8},{4,12},{8,16},{12,20},{16,24},{20,28},{1,9},{5,13},{9,17},{1... | collective-permute-start | bytes 417800 | tf_op jit(solution)/shard_map/ppermute | solution.py:284
  257.1 9.8 %collective-permute-start.4 = (bf16[272,256]{1,0:T(8,128)(2,1)}, bf16[272,256]{1,0:T(8,128)(2,1)S(1)}, u32[]{:S(2)}, u32[]{:S(2)}) collective-permute-start(bf16[272,256]{1,0:T(8,128)(2,1)} %merge.4.later_ref), channel_id=1, source_target_pairs={{0,16},{4,20},{8,24},{12,28},{1,17},{5,21},{9,25},{13,29},{2,18},{... | collective-permute-start | bytes 417800 | tf_op jit(solution)/shard_map/ppermute | solution.py:284
  (12 other events, 35.2 us)
